TPU v7x, 256 devices: a whole 4x4x8 slice. The times are simulated.
256 devices in a mesh: ep: 64 (over z, x, core), tp: 4 (over y).
Axes of the slice: x: 4, y: 4, z: 8, core: 2. Of those that a mesh axis runs over, the one named last changes fastest.
Arguments:
- queries: bfloat16 [32768, 1024], P('ep', 'tp'), may hold values from -6 to 6
- mixer_key_rows: bfloat16 [32768, 1024], P('ep', 'tp'), may hold values from -6 to 6
- mixer_value_rows: bfloat16 [32768, 2048], P('ep', 'tp'), may hold values from -6 to 6
- log_input_gate: float32 [8, 32768], P('tp', 'ep'), may hold values from -6 to 136
- forget_gate_logits: float32 [8, 32768], P('tp', 'ep'), may hold values from 1 to 20
- extra_log_decay: float32 [8, 32768], P('tp', 'ep'), may hold values from -1.4 to 0
- head_norm_gain: float32 [2048], P('tp'), may hold values from 0.1 to 1.9
- mixer_output_weight: bfloat16 [2048, 2048], P('tp'), may hold values from -0.125 to 0.125
- expert_input_rows: bfloat16 [16384, 2048], P(('ep', 'tp')), may hold values from -6 to 6
- expert_norm_gain: float32 [2048], replicated, may hold values from 0.1 to 1.9
- routes: int32 [16384, 3], P(('ep', 'tp')), may hold values from 0 to 63, all different within a row; in each aligned block of 64 rows (0 to 63, 64 to 127, ...) at most 6 rows name the same one
- router_picked_scores: float32 [16384, 3], P(('ep', 'tp')), may hold values from 0.1 to 1
- expert_gate_weight: bfloat16 [64, 2048, 1024], P('ep', None, 'tp'), may hold values from -0.125 to 0.125
- expert_up_weight: bfloat16 [64, 2048, 1024], P('ep', None, 'tp'), may hold values from -0.125 to 0.125
- expert_down_weight: bfloat16 [64, 2048, 1024], P('ep', None, 'tp'), may hold values from -0.1875 to 0.1875
Outputs:
- mixer_output: bfloat16 [32768, 2048], P(('ep', 'tp'))
- expert_out: bfloat16 [16384, 2048], P(('ep', 'tp'))
Inputs may be any that keep to these rules, and one draw needn't show every extreme that they name: `routes`: in each aligned block of 64 rows, the rows of one device, no expert is named by more than 6 rows, a bound that some block reaches; a row names 3 different experts.
All inputs are finite; a program needn't handle non-finite values.
Results may differ from a plain program's by a relative error of at most 0.014.
Values may be sent and summed in bfloat16 or wider, within the bound.
No kernel may reach another device: no remote copies, remote signals or barrier semaphores. Data moves between devices by JAX's collectives and lax.ppermute only.
A program may use at most 128 MiB of HBM per device.

v0:
```python
import jax
import jax.numpy as jnp
from jax import lax
from jax.sharding import Mesh
from jax.sharding import PartitionSpec as P

BLOCK = 64
EP = ("ep_0", "ep_1", "ep_2")
EP_TP = ("ep_0", "ep_1", "ep_2", "tp")


EPSILON = 1e-06
LOW_LEVEL = -1e30


def neutral_like(shard, identity):
    return jax.tree.map(
        lambda part, zero: jnp.zeros_like(part) + jnp.asarray(zero, part.dtype), shard, identity
    )


def all_in_one(shard, axis):
    leaves = jax.tree.leaves(shard)
    turns = sorted(range(len(leaves)), key=lambda k: -leaves[k].size)
    width = (1, *leaves[turns[0]].shape)[-1]
    lines = [
        jnp.pad(leaves[k].reshape(-1), (0, -leaves[k].size % width)).reshape(-1, width)
        for k in turns
    ]
    both, at, found = (lax.all_gather(jnp.concatenate(lines), axis), 0, {})
    for k, line in zip(turns, lines):
        share = both[:, at : at + len(line)].reshape(len(both), -1)
        found[k] = share[:, : leaves[k].size].reshape(-1, *leaves[k].shape)
        at += len(line)
    numbers = iter(range(len(leaves)))
    return jax.tree.map(lambda _: found[next(numbers)], shard)


def prefix_by_axis(shard, axes, combine, identity):
    before = start = neutral_like(shard, identity)
    total = shard
    for axis in reversed(axes):
        devices, index = (lax.axis_size(axis), lax.axis_index(axis))
        pieces = all_in_one(total, axis)
        inside, total = (start, start)
        for k in range(devices):
            passed = k < index
            total = combine(total, jax.tree.map(lambda part: part[k], pieces))
            inside = jax.tree.map(lambda new, old: jnp.where(passed, new, old), total, inside)
        before = combine(inside, before)
    return before


def side_by_side(arrays, axis, dim, along):
    ends, at = ([], 0)
    for a in arrays[:-1]:
        at += a.shape[along]
        ends.append(at)
    both = jnp.concatenate(arrays, axis=along)
    return tuple(jnp.split(lax.all_gather(both, axis, axis=dim, tiled=True), ends, axis=along))


def join_states(earlier, later):
    early_memory, early_level, early_decay = earlier
    late_memory, late_level, late_decay = later
    highest = jnp.maximum(late_decay + early_level, late_level)
    memory = (
        jnp.exp(late_decay + early_level - highest)[..., None, None] * early_memory
        + jnp.exp(late_level - highest)[..., None, None] * late_memory
    )
    return (memory, highest, early_decay + late_decay)


def mixer_part(
    queries,
    mixer_key_rows,
    mixer_value_rows,
    log_input_gate,
    forget_gate_logits,
    extra_log_decay,
    head_norm_gain,
    mixer_output_weight,
):
    head_count, token_count = log_input_gate.shape
    block_count = token_count // BLOCK
    key_width = queries.shape[1] // head_count
    value_width = mixer_value_rows.shape[1] // head_count
    precise = lax.Precision.HIGHEST

    def to_blocks(tensor, lane):
        return (
            tensor.reshape(block_count, BLOCK, head_count, lane)
            .transpose(2, 0, 1, 3)
            .astype(jnp.float32)
        )

    query_f = to_blocks(queries, key_width) * key_width ** (-0.5)
    key_f = to_blocks(mixer_key_rows, key_width)
    value_f = to_blocks(mixer_value_rows, value_width)
    forget_log_value = (jax.nn.log_sigmoid(forget_gate_logits) + extra_log_decay).reshape(
        head_count, block_count, BLOCK
    )
    gate_in = log_input_gate.reshape(head_count, block_count, BLOCK)
    cumulative = jnp.cumsum(forget_log_value, axis=-1)
    span_decay = cumulative[..., -1]
    gap = span_decay[..., None] - cumulative + gate_in
    local_level = jnp.max(gap, axis=-1)
    weighted = key_f * jnp.exp(gap - local_level[..., None])[..., None]
    local_memory = jnp.einsum("hnsd,hnse->hnde", weighted, value_f, precision=precise)
    inclusive = lax.associative_scan(join_states, (local_memory, local_level, span_decay), axis=1)
    device_state = (inclusive[0][:, -1], inclusive[1][:, -1], inclusive[2][:, -1])
    identity = (
        jnp.zeros_like(device_state[0]),
        jnp.full_like(device_state[1], LOW_LEVEL),
        jnp.zeros_like(device_state[2]),
    )
    prefix = prefix_by_axis(device_state, EP, join_states, identity)
    shifted = (
        jnp.concatenate([jnp.zeros_like(inclusive[0][:, :1]), inclusive[0][:, :-1]], axis=1),
        jnp.concatenate(
            [jnp.full_like(inclusive[1][:, :1], LOW_LEVEL), inclusive[1][:, :-1]], axis=1
        ),
        jnp.concatenate([jnp.zeros_like(inclusive[2][:, :1]), inclusive[2][:, :-1]], axis=1),
    )
    entry_memory, entry_level, _ = join_states(
        (prefix[0][:, None], prefix[1][:, None], prefix[2][:, None]), shifted
    )
    causal_mask = jnp.tril(jnp.ones((BLOCK, BLOCK), dtype=bool))
    within = cumulative[..., :, None] - cumulative[..., None, :] + gate_in[..., None, :]
    within = jnp.where(causal_mask, within, -jnp.inf)
    carried = cumulative + entry_level[..., None]
    row_max = jnp.maximum(carried, jnp.max(within, axis=-1))
    scores = jnp.einsum("hnjd,hnsd->hnjs", query_f, key_f, precision=precise) * jnp.exp(
        within - row_max[..., None]
    )
    cell = jnp.einsum("hnjs,hnse->hnje", scores, value_f, precision=precise)
    cell = cell + jnp.exp(carried - row_max)[..., None] * jnp.einsum(
        "hnjd,hnde->hnje", query_f, entry_memory, precision=precise
    )
    normed = cell * lax.rsqrt(jnp.mean(cell * cell, axis=-1, keepdims=True) + EPSILON)
    normed = normed.transpose(1, 2, 0, 3).reshape(token_count, head_count * value_width)
    normed = (normed * head_norm_gain).astype(jnp.bfloat16)
    return lax.psum_scatter(
        jnp.dot(normed, mixer_output_weight, preferred_element_type=jnp.float32).astype(
            jnp.bfloat16
        ),
        "tp",
        scatter_dimension=0,
        tiled=True,
    )


def experts_part(
    expert_input_rows,
    expert_norm_gain,
    routes,
    router_picked_scores,
    expert_gate_weight,
    expert_up_weight,
    expert_down_weight,
):
    row_total, model_width = expert_input_rows.shape
    pick_count = routes.shape[1]
    local_experts = expert_gate_weight.shape[0]
    expert_count = local_experts * lax.axis_size(EP)
    capacity = 2 * row_total * pick_count // expert_count
    inputs_f = expert_input_rows.astype(jnp.float32)
    normed = (
        inputs_f
        * lax.rsqrt(jnp.mean(inputs_f * inputs_f, axis=-1, keepdims=True) + EPSILON)
        * expert_norm_gain
    ).astype(jnp.bfloat16)
    share = router_picked_scores / jnp.sum(router_picked_scores, axis=-1, keepdims=True)
    flat_routes = routes.reshape(-1)
    onehot = (flat_routes[:, None] == jnp.arange(expert_count, dtype=jnp.int32)[None, :]).astype(
        jnp.int32
    )
    before = jnp.sum((jnp.cumsum(onehot, axis=0) - onehot) * onehot, axis=1)
    slot_index = flat_routes * capacity + before
    row_owner = jnp.arange(row_total * pick_count, dtype=jnp.int32) // pick_count
    slot_owner = (
        jnp.full((expert_count * capacity,), row_total, jnp.int32).at[slot_index].set(row_owner)
    )
    padded = jnp.concatenate([normed, jnp.zeros((1, model_width), jnp.bfloat16)], axis=0)
    outgoing = padded[slot_owner].reshape(expert_count, capacity, model_width)
    full_gate, full_up, full_down = side_by_side(
        (expert_gate_weight, expert_up_weight, expert_down_weight), "tp", 2, 0
    )
    arrived = lax.all_to_all(outgoing, EP, split_axis=0, concat_axis=0, tiled=True)
    source_count = arrived.shape[0] // local_experts
    item_count = arrived.shape[1]
    stacked = arrived.reshape(source_count, local_experts, item_count, model_width)
    stacked = stacked.transpose(0, 2, 1, 3).reshape(
        source_count * item_count, local_experts, model_width
    )
    gate_val = jnp.einsum("red,edf->ref", stacked, full_gate, preferred_element_type=jnp.float32)
    up_val = jnp.einsum("red,edf->ref", stacked, full_up, preferred_element_type=jnp.float32)
    hidden = (jax.nn.silu(gate_val) * up_val).astype(jnp.bfloat16)
    result = jnp.einsum(
        "ref,edf->red", hidden, full_down, preferred_element_type=jnp.float32
    ).astype(jnp.bfloat16)
    send_result = result
    source_count = arrived.shape[0] // local_experts
    item_count = arrived.shape[1]
    send_result = send_result.reshape(
        source_count, item_count, local_experts, model_width
    ).transpose(0, 2, 1, 3)
    send_result = send_result.reshape(source_count * local_experts, item_count, model_width)
    returned = lax.all_to_all(send_result, EP, split_axis=0, concat_axis=0, tiled=True)
    picked = returned.reshape(expert_count * capacity, model_width)[slot_index]
    picked = picked.reshape(row_total, pick_count, model_width)
    return jnp.sum(share[..., None] * picked.astype(jnp.float32), axis=1).astype(jnp.bfloat16)


def shards(
    queries,
    mixer_key_rows,
    mixer_value_rows,
    log_input_gate,
    forget_gate_logits,
    extra_log_decay,
    head_norm_gain,
    mixer_output_weight,
    expert_input_rows,
    expert_norm_gain,
    routes,
    router_picked_scores,
    expert_gate_weight,
    expert_up_weight,
    expert_down_weight,
):
    mixer_output = mixer_part(
        queries,
        mixer_key_rows,
        mixer_value_rows,
        log_input_gate,
        forget_gate_logits,
        extra_log_decay,
        head_norm_gain,
        mixer_output_weight,
    )
    expert_out = experts_part(
        expert_input_rows,
        expert_norm_gain,
        routes,
        router_picked_scores,
        expert_gate_weight,
        expert_up_weight,
        expert_down_weight,
    )
    return (mixer_output, expert_out)


def solution(mesh):
    split = Mesh(mesh.devices.reshape(8, 4, 2, mesh.shape["tp"]), ("ep_0", "ep_1", "ep_2", "tp"))
    in_specs = (
        P(EP, "tp"),
        P(EP, "tp"),
        P(EP, "tp"),
        P("tp", EP),
        P("tp", EP),
        P("tp", EP),
        P("tp"),
        P("tp", None),
        P(EP_TP, None),
        P(),
        P(EP_TP, None),
        P(EP_TP, None),
        P(EP, None, "tp"),
        P(EP, None, "tp"),
        P(EP, None, "tp"),
    )
    out_specs = (P(EP_TP, None), P(EP_TP, None))
    return jax.shard_map(
        shards, mesh=split, in_specs=in_specs, out_specs=out_specs, check_vma=False
    )
```

profile of v0, /device:TPU:2, one launch (start us, length us, event | category | flops | bytes accessed | tf_op | source)
XLA Modules:
  0.0 368.9 jit_solution(13699446728572647594)
XLA Ops:
  22.2 4.1 %pad.96 = f32[2,4,128,256]{3,2,1,0:T(8,128)} pad(f32[2,2,128,256]{3,2,1,0:T(8,128)} %pad_maximum_fusion.2, f32[]{:T(128)} %constant.28.clone.1), padding=0_0_0x0_1_1x0_0_0x0_0_0 | pad | bytes 1572868 | tf_op jit(solution)/shard_map/pad | solution.py:110
  26.8 2.3 add.1089
  29.2 6.5 %pad.183 = f32[2,8,128,256]{3,2,1,0:T(8,128)} pad(f32[2,4,128,256]{3,2,1,0:T(8,128)} %add.1089, f32[]{:T(128)} %constant.28.clone.1), padding=0_0_0x1_0_1x0_0_0x0_0_0 | pad | bytes 3145732
  38.0 4.0 %pad.98 = f32[2,8,128,256]{3,2,1,0:T(8,128)} pad(f32[2,4,128,256]{3,2,1,0:T(8,128)S(1)} %pad_maximum_fusion.1, f32[]{:T(128)} %constant.28.clone.1), padding=0_0_0x0_1_1x0_0_0x0_0_0 | pad | bytes 3145732 | tf_op jit(solution)/shard_map/pad | solution.py:110
  43.1 2.2 all-gather.3
  47.2 28.6 %all-gather.12.cloned.1.call-done = f32[4,258,256]{2,1,0:T(8,128)} async-done(((f32[1,258,256]{2,1,0:T(8,128)}), f32[4,258,256]{2,1,0:T(8,128)}) %all-gather.12.cloned.1.call-update) | async-done | bytes 1056784 | tf_op jit(solution)/shard_map/all_gather | solution.py:30
  79.7 3.8 %pad_maximum_fusion = bf16[3,2048,256]{2,1,0:T(8,128)(2,1)} fusion(bf16[1,2048,256]{2,1,0:T(8,128)(2,1)} %param.29, bf16[1,2048,256]{2,1,0:T(8,128)(2,1)} %param.28, bf16[1,2048,256]{2,1,0:T(8,128)(2,1)} %param.27), kind=kLoop, calls=%fused_computation.9 | loop fusion | flops 3145728 | bytes 6291456 | tf_op jit(solution)/shard_map/concatenate | solution.py:59
  90.0 3.1 gather_fusion
  93.1 3.7 reshape.1686
  96.8 11.0 %all-to-all-start = ((bf16[64,6,2048]{2,1,0:T(8,128)(2,1)}), bf16[64,6,2048]{2,1,0:T(8,128)(2,1)}, u32[]{:S(2)}, u32[]{:S(2)}) async-start(bf16[64,6,2048]{2,1,0:T(8,128)(2,1)} %reshape.1686), calls=%async_computation.1 | async-start | bytes 4194304 | tf_op jit(solution)/shard_map/all_to_all | solution.py:189
  107.9 4.0 %pad.138 = f32[2,7,128,256]{3,2,1,0:T(8,128)} pad(f32[2,4,128,256]{3,2,1,0:T(8,128)S(1)} %pad_maximum_fusion.1, f32[]{:T(128)} %constant.28.clone.1), padding=0_0_0x0_0_1x0_0_0x0_0_0 | pad | bytes 2883588 | tf_op jit(solution)/shard_map/slice | solution.py:119
  116.2 3.7 %slice_add_fusion.8 = f32[2,7,128,256]{3,2,1,0:T(8,128)} fusion(f32[2,7,128,256]{3,2,1,0:T(8,128)} %pad.138, f32[2,8,128,256]{3,2,1,0:T(8,128)} %pad.183), kind=kLoop, calls=%fused_computation.314 | loop fusion | flops 458752 | bytes 5505024 | tf_op jit(solution)/shard_map/add | solution.py:110
  120.9 44.1 %all-to-all-done = bf16[64,6,2048]{2,1,0:T(8,128)(2,1)} async-done(((bf16[64,6,2048]{2,1,0:T(8,128)(2,1)}), bf16[64,6,2048]{2,1,0:T(8,128)(2,1)}, u32[]{:S(2)}, u32[]{:S(2)}) %all-to-all-start) | async-done | bytes 1572896 | tf_op jit(solution)/shard_map/all_to_all | solution.py:189
  165.0 3.7 %reshape.1687 = bf16[384,2048]{1,0:T(8,128)(2,1)} reshape(bf16[64,6,2048]{2,1,0:T(8,128)(2,1)} %all-to-all-done) | data formatting | bytes 3145728 | tf_op jit(solution)/shard_map/reshape.68
  178.0 2.6 convolution_convert_fusion
  180.6 87.1 %all-gather.10.cloned.1.call-done = bf16[3,2048,1024]{2,1,0:T(8,128)(2,1)} async-done(((bf16[3,2048,256]{2,1,0:T(8,128)(2,1)}), bf16[3,2048,1024]{2,1,0:T(8,128)(2,1)}) %all-gather.10.cloned.1.call-update) | async-done | bytes 12582928 | tf_op jit(solution)/shard_map/all_gather | solution.py:60
  267.7 6.2 %fusion.1 = f32[1024,384]{1,0:T(8,128)} fusion(bf16[384,2048]{1,0:T(8,128)(2,1)} %reshape.1687, bf16[3,2048,1024]{2,1,0:T(8,128)(2,1)} %all-gather.10.cloned.1.call-done), kind=kOutput, calls=%fused_computation.6 | convolution fusion | flops 1610612736 | bytes 7340032 | tf_op jit(solution)/shard_map/red,edf->ref/dot_general | solution.py:196
  273.9 9.9 %fusion.4 = bf16[384,1,2048]{2,0,1:T(8,128)(2,1)} fusion(bf16[3,2048,1024]{2,1,0:T(8,128)(2,1)} %all-gather.10.cloned.1.call-done, bf16[384,2048]{1,0:T(8,128)(2,1)} %reshape.1687, f32[1024,384]{1,0:T(8,128)} %fusion.1), kind=kOutput, calls=%fused_computation.12 | convolution fusion | flops 3224371200 | bytes 13107200 | tf_op jit(solution)/shard_map/ref,edf->red/dot_general | solution.py:199
  283.8 3.7 reshape_transpose_reshape.4
  287.5 10.9 %all-to-all-start.1 = ((bf16[64,6,2048]{2,1,0:T(8,128)(2,1)}), bf16[64,6,2048]{2,1,0:T(8,128)(2,1)}, u32[]{:S(2)}, u32[]{:S(2)}) async-start(bf16[64,6,2048]{2,1,0:T(8,128)(2,1)} %reshape_transpose_reshape.4), calls=%async_computation.2 | async-start | bytes 4194304 | tf_op jit(solution)/shard_map/all_to_all | solution.py:209
  298.5 51.0 %all-to-all-done.1 = bf16[64,6,2048]{2,1,0:T(8,128)(2,1)} async-done(((bf16[64,6,2048]{2,1,0:T(8,128)(2,1)}), bf16[64,6,2048]{2,1,0:T(8,128)(2,1)}, u32[]{:S(2)}, u32[]{:S(2)}) %all-to-all-start.1) | async-done | bytes 1572896 | tf_op jit(solution)/shard_map/all_to_all | solution.py:209
  349.5 3.7 %reshape.1690 = bf16[384,2048]{1,0:T(8,128)(2,1)} reshape(bf16[64,6,2048]{2,1,0:T(8,128)(2,1)} %all-to-all-done.1) | data formatting | bytes 3145728 | tf_op jit(solution)/shard_map/reshape | solution.py:210
  353.2 3.5 gather_fusion.1
  358.5 3.9 %multiply_reduce_fusion = bf16[64,2048]{1,0:T(8,128)(2,1)} fusion(f32[64,3,2048]{2,1,0:T(4,128)} %reshape.1692, f32[64,3]{1,0:T(8,128)S(1)} %copy.34), kind=kLoop, calls=%fused_computation.13 | loop fusion | flops 655360 | bytes 1835776 | tf_op jit(solution)/shard_map/reduce_sum | solution.py:212
  (277 shorter events, 46.5 us)
Async XLA Ops:
  7.2 170.8 %copy-start = (bf16[512,2048]{1,0:T(8,128)(2,1)S(1)}, bf16[512,2048]{1,0:T(8,128)(2,1)}, u32[]{:S(2)}) copy-start(bf16[512,2048]{1,0:T(8,128)(2,1)} %param.22) | copy-start | bytes 6291460
  7.2 68.6 %all-gather.12.cloned.1.call-start = ((), (), s32[]{:S(2)}) async-start(), calls=%async_computation.5 | async-start | bytes 1351680 | tf_op jit(solution)/shard_map/all_gather | solution.py:30
  45.4 34.3 %copy-start.20 = (f32[2]{0:T(128)}, f32[2]{0:T(128)S(1)}, u32[]{:S(2)}) copy-start(f32[2]{0:T(128)S(1)} %get-tuple-element.29) | copy-start | bytes 28
  45.4 31.2 %copy-start.38 = (f32[2]{0:T(128)}, f32[2]{0:T(128)S(1)}, u32[]{:S(2)}) copy-start(f32[2]{0:T(128)S(1)} %get-tuple-element.111) | copy-start | bytes 28
  45.5 31.2 %copy-start.40 = (f32[2]{0:T(128)}, f32[2]{0:T(128)S(1)}, u32[]{:S(2)}) copy-start(f32[2]{0:T(128)S(1)} %get-tuple-element.112) | copy-start | bytes 28
  45.5 34.2 %copy-start.22 = (f32[2]{0:T(128)}, f32[2]{0:T(128)S(1)}, u32[]{:S(2)}) copy-start(f32[2]{0:T(128)S(1)} %get-tuple-element.88) | copy-start | bytes 28
  47.1 121.6 %all-gather.14.cloned.1.call-start = ((), (), s32[]{:S(2)}) async-start(), calls=%async_computation.6 | async-start | bytes 2433024 | tf_op jit(solution)/shard_map/all_gather | solution.py:30
  76.6 6.9 %copy-start.26 = (f32[2]{0:T(128)}, f32[2]{0:T(128)S(1)}, u32[]{:S(2)}) copy-start(f32[2]{0:T(128)S(1)} %get-tuple-element.24) | copy-start | bytes 28
  76.6 6.9 %copy-start.28 = (f32[2]{0:T(128)}, f32[2]{0:T(128)S(1)}, u32[]{:S(2)}) copy-start(f32[2]{0:T(128)S(1)} %get-tuple-element.25) | copy-start | bytes 28
  76.7 6.9 %copy-start.30 = (f32[2]{0:T(128)}, f32[2]{0:T(128)S(1)}, u32[]{:S(2)}) copy-start(f32[2]{0:T(128)S(1)} %get-tuple-element.26) | copy-start | bytes 28
  76.7 6.9 %copy-start.56 = (f32[2]{0:T(128)}, f32[2]{0:T(128)S(1)}, u32[]{:S(2)}) copy-start(f32[2]{0:T(128)S(1)} %get-tuple-element.22) | copy-start | bytes 28
  79.6 188.1 %all-gather.10.cloned.1.call-start = ((), (), s32[]{:S(2)}) async-start(), calls=%async_computation.4 | async-start | bytes 15728640 | tf_op jit(solution)/shard_map/all_gather | solution.py:60
  96.8 68.2 %all-to-all-start = ((bf16[64,6,2048]{2,1,0:T(8,128)(2,1)}), bf16[64,6,2048]{2,1,0:T(8,128)(2,1)}, u32[]{:S(2)}, u32[]{:S(2)}) async-start(bf16[64,6,2048]{2,1,0:T(8,128)(2,1)} %reshape.1686), calls=%async_computation.1 | async-start | bytes 4194304 | tf_op jit(solution)/shard_map/all_to_all | solution.py:189
  107.8 254.6 %reduce-scatter.2.cloned.1.call-start = ((), (), s32[]{:S(2)}) async-start(), calls=%async_computation.3 | async-start | bytes 2621440 | tf_op jit(solution)/shard_map/reduce_scatter | solution.py:143
  120.8 48.9 %copy-start.23 = (f32[2]{0:T(128)S(1)}, f32[2]{0:T(128)}, u32[]{:S(2)}) copy-start(f32[2]{0:T(128)} %copy-done.22) | copy-start | bytes 28
  120.8 48.9 %copy-start.25 = (f32[2]{0:T(128)S(1)}, f32[2]{0:T(128)}, u32[]{:S(2)}) copy-start(f32[2]{0:T(128)} %copy-done.24) | copy-start | bytes 28
  120.9 48.9 %copy-start.21 = (f32[2]{0:T(128)S(1)}, f32[2]{0:T(128)}, u32[]{:S(2)}) copy-start(f32[2]{0:T(128)} %copy-done.20) | copy-start | bytes 28
  120.9 48.9 %copy-start.27 = (f32[2]{0:T(128)S(1)}, f32[2]{0:T(128)}, u32[]{:S(2)}) copy-start(f32[2]{0:T(128)} %copy-done.26) | copy-start | bytes 28
  120.9 48.9 %copy-start.29 = (f32[2]{0:T(128)S(1)}, f32[2]{0:T(128)}, u32[]{:S(2)}) copy-start(f32[2]{0:T(128)} %copy-done.28) | copy-start | bytes 28
  120.9 48.9 %copy-start.31 = (f32[2]{0:T(128)S(1)}, f32[2]{0:T(128)}, u32[]{:S(2)}) copy-start(f32[2]{0:T(128)} %copy-done.30) | copy-start | bytes 28
  120.9 48.9 %copy-start.33 = (f32[2,8]{1,0:T(2,128)S(1)}, f32[2,8]{1,0:T(2,128)}, u32[]{:S(2)}) copy-start(f32[2,8]{1,0:T(2,128)} %copy-done.32) | copy-start | bytes 196
  120.9 49.2 %copy-start.12 = (bf16[8,64,2,128]{3,2,1,0:T(2,128)(2,1)S(1)}, bf16[8,64,2,128]{3,2,1,0:T(2,128)(2,1)}, u32[]{:S(2)}) copy-start(bf16[8,64,2,128]{3,2,1,0:T(2,128)(2,1)} %copy-done.11) | copy-start | bytes 786436
  287.5 10.9 %copy-start.19 = (f32[64,3]{0,1:T(4,128)S(1)}, f32[64,3]{0,1:T(4,128)}, u32[]{:S(2)}) copy-start(f32[64,3]{0,1:T(4,128)} %param.26) | copy-start | bytes 2308
  287.5 62.0 %all-to-all-start.1 = ((bf16[64,6,2048]{2,1,0:T(8,128)(2,1)}), bf16[64,6,2048]{2,1,0:T(8,128)(2,1)}, u32[]{:S(2)}, u32[]{:S(2)}) async-start(bf16[64,6,2048]{2,1,0:T(8,128)(2,1)} %reshape_transpose_reshape.4), calls=%async_computation.2 | async-start | bytes 4194304 | tf_op jit(solution)/shard_map/all_to_all | solution.py:209
  (42 other events, 117.6 us)
Sparse Core Ops, SparseCore 0:
  47.2 28.4 all-gather.11
  79.7 61.4 all-gather.13
  143.0 124.6 all-gather.9
  270.7 32.5 reduce-scatter.1
where the time goes:
time: 370 us; the launch traced here: 369 us
  waiting for transfers between devices  211 us (57%)
  local copies, waits for them, and re-layouts  63.4 us (17%)
  other arithmetic  32.4 us (9%)
  matrix products  23 us (6%)
  starting transfers between devices  22.1 us (6%)
  between operations  15 us (4%)
    all_gather x1, waiting for transfers between devices, side_by_side(): lax.all_gather(both, axis, axis=dim, tiled=True)  87.1 us
    all_to_all x1, waiting for transfers between devices, experts_part(): lax.all_to_all(send_result, EP, split_axis=0, concat_axis=0, tiled=True)  51 us
    all_to_all x1, waiting for transfers between devices, experts_part(): lax.all_to_all(outgoing, EP, split_axis=0, concat_axis=0, tiled=True)  44.1 us
    all_gather x2, waiting for transfers between devices, all_in_one(): both, at, found = (lax.all_gather(jnp.concatenate(lines), axis), 0, {})  28.6 us
    all_to_all x1, starting transfers between devices, experts_part(): lax.all_to_all(outgoing, EP, split_axis=0, concat_axis=0, tiled=True)  11 us
    all_to_all x1, starting transfers between devices, experts_part(): lax.all_to_all(send_result, EP, split_axis=0, concat_axis=0, tiled=True)  10.9 us
    pad x11, local copies, waits for them, and re-layouts, mixer_part(): lax.associative_scan(join_states, (local_memory, local_level, span_decay)...  10.8 us
    unnamed x127, local copies, waits for them, and re-layouts  10.1 us
  transfers between devices with their start and end apart: 6, of which 4 were waited for; matrix products, arithmetic and copies ran while one was open for 21% of the time, Pallas kernels for 0%

commit v1 on v0

v1 whole, which is shorter than its diff:
```python
import jax
import jax.numpy as jnp
from jax import lax
from jax.experimental import pallas as pl
from jax.experimental.pallas import tpu as pltpu
from jax.sharding import Mesh
from jax.sharding import PartitionSpec as P


EP = ("ep_0", "ep_1", "ep_2")
EP_TP = ("ep_0", "ep_1", "ep_2", "tp")
EPSILON = 1e-06
LOW_LEVEL = -1e30
F32 = jnp.float32
BF16 = jnp.bfloat16

N_EP = 64
N_TP = 4
TOK = 512
KEY = 128
VAL = 256
WIDTH = 2048
QUARTER = 256
ROWS = 64
CAP = 6
PIECES = 8
PIECE = 256
MSG = CAP * PIECES
EXPERTS = 64
GROUP = 8
BLOCKS = 4
PART = WIDTH // BLOCKS

PARAMS = pltpu.CompilerParams(vmem_limit_bytes=56 * 1024 * 1024)
SMALL = pltpu.CompilerParams(vmem_limit_bytes=40 * 1024 * 1024)


def iota(shape, dim):
    return lax.broadcasted_iota(jnp.int32, shape, dim)


def dot(a, b):
    return jnp.dot(a, b, preferred_element_type=F32)


def dot_nt(a, b):
    return lax.dot_general(a, b, (((1,), (1,)), ((), ())), preferred_element_type=F32)


def in_vmem(x):
    return pltpu.with_memory_space_constraint(x, pltpu.VMEM)


def two_parts(x):
    high = x.astype(BF16).astype(F32)
    return high, (x - high).astype(BF16).astype(F32)


def three_parts(x):
    high = x.astype(BF16).astype(F32)
    rest = x - high
    middle = rest.astype(BF16).astype(F32)
    return high, middle, (rest - middle).astype(BF16).astype(F32)


def state_body(keys, values, gate_in, log_forget, state, gaps):
    upper = (iota((TOK, TOK), 0) <= iota((TOK, TOK), 1)).astype(F32).astype(BF16)
    odd = (iota((8, TOK), 0) & 1) == 1
    decay = jnp.where(odd, log_forget[1:2], log_forget[0:1])
    parts = jnp.concatenate(three_parts(decay), axis=0).astype(BF16)
    sums = dot(parts, upper)
    total = sums[0:8] + sums[8:16] + sums[16:24]
    gap = jnp.where(odd, gate_in[1:2], gate_in[0:1]) - total
    gaps[...] = gap
    blocks = []
    lane = iota((8, 128), 1)
    row = iota((8, 128), 0)
    scalars = jnp.zeros((8, 128), F32)
    for h in range(2):
        own = gap[h : h + 1]
        highest = jnp.max(own, axis=1, keepdims=True)
        key_t = keys[:, h * KEY : (h + 1) * KEY].astype(F32).T
        weighted = key_t * jnp.exp(own - highest)
        own_values = values[:, h * VAL : (h + 1) * VAL]
        memory = sum(dot(part.astype(BF16), own_values) for part in two_parts(weighted))
        blocks += [memory[:, :128], memory[:, 128:]]
        for n, part in enumerate(three_parts(highest) + three_parts(total[h : h + 1, TOK - 1 : TOK])):
            scalars = scalars + jnp.where((lane == 6 * h + n) & (row == 0), part, 0.0)
    stacked = jnp.concatenate(blocks, axis=0).reshape(N_EP, 8, 128)
    spread = jnp.broadcast_to(scalars[None], (N_EP, 8, 128))
    high, low = two_parts(stacked)
    upper_rows = jnp.concatenate([high, spread], axis=2)
    lower_rows = jnp.concatenate([low, jnp.zeros_like(spread)], axis=2)
    state[...] = jnp.concatenate([upper_rows, lower_rows], axis=1).astype(BF16)


def prefix_body(index, arrived, prefix, level):
    place = index[0]
    full = arrived[:, MSG:, :].astype(F32)
    high = full[:, :8, :128].reshape(N_EP * 8, 128).astype(BF16)
    low = full[:, 8:, :128].reshape(N_EP * 8, 128).astype(BF16)
    scalars = jnp.sum(full[:, :8, 128:], axis=1)
    row, col = iota((N_EP, N_EP), 0), iota((N_EP, N_EP), 1)
    earlier = col < row
    factors = []
    own_row = iota((N_EP, 1), 0) == place
    out_row = iota((8, 128), 0)
    levels = jnp.zeros((8, 128), F32)
    for h in range(2):
        cols = [scalars[:, 6 * h + n : 6 * h + n + 1] for n in range(6)]
        highest = cols[0] + cols[1] + cols[2]
        decay = cols[3] + cols[4] + cols[5]
        highest_row = jnp.sum(jnp.where(row == col, highest, 0.0), axis=0, keepdims=True)
        between = jnp.dot(
            earlier.astype(F32),
            jnp.where(row >= col, decay, 0.0),
            precision=lax.Precision.HIGHEST,
            preferred_element_type=F32,
        )
        exponent = jnp.where(earlier, highest_row + between, -3e38)
        top = jnp.maximum(jnp.max(exponent, axis=1, keepdims=True), LOW_LEVEL)
        factors.append(jnp.where(earlier, jnp.exp(exponent - top), 0.0))
        mine = jnp.sum(jnp.where(own_row, top, 0.0), axis=0, keepdims=True)
        levels = levels + jnp.where(out_row == h, mine, 0.0)
    level[...] = levels
    factor = jnp.where(place >= N_EP // 2, factors[1], factors[0]).astype(BF16)
    wide = N_EP * 8
    spread = ((iota((wide, N_EP), 0) >> 3) == iota((wide, N_EP), 1)).astype(F32).astype(BF16)
    spread_t = (iota((N_EP, wide), 0) == (iota((N_EP, wide), 1) >> 3)).astype(F32).astype(BF16)
    repeated = dot(dot(spread, factor).astype(BF16), spread_t)
    same = (iota((wide, wide), 0) & 7) == (iota((wide, wide), 1) & 7)
    mixing = jnp.where(same, repeated, 0.0).astype(BF16)
    mixed = (dot(mixing, high) + dot(mixing, low)).reshape(N_EP, 8, 128)
    prefix[...] = jnp.concatenate(two_parts(mixed), axis=1).astype(BF16)


def cell_body(index, queries, keys, values, gaps, prefix, level, gain, weight, out_0, out_1, out_2, out_3, normed, partial):
    slices = prefix[...].astype(F32)
    halves = [slices[:, :8].reshape(N_EP * 8, 128), slices[:, 8:].reshape(N_EP * 8, 128)]
    causal = iota((TOK, TOK), 1) <= iota((TOK, TOK), 0)
    for h in range(2):
        query = queries[:, h * KEY : (h + 1) * KEY]
        recalled = 0.0
        for part in halves:
            columns = [part[256 * h : 256 * h + 128], part[256 * h + 128 : 256 * h + 256]]
            recalled = recalled + dot(query, jnp.concatenate(columns, axis=1).astype(BF16))
        exponent = jnp.where(causal, gaps[h : h + 1, :], -jnp.inf)
        carried = level[h : h + 1, 0:1]
        top = jnp.maximum(jnp.max(exponent, axis=1, keepdims=True), carried)
        scores = dot_nt(query, keys[:, h * KEY : (h + 1) * KEY]) * (KEY**-0.5)
        scores = scores * jnp.exp(exponent - top)
        cell = dot(scores.astype(BF16), values[:, h * VAL : (h + 1) * VAL])
        cell = cell + (jnp.exp(carried - top) * KEY**-0.5) * recalled
        scale = lax.rsqrt(jnp.mean(cell * cell, axis=1, keepdims=True) + EPSILON)
        normed[:, h * VAL : (h + 1) * VAL] = (cell * scale * gain[:, h * VAL : (h + 1) * VAL]).astype(BF16)
    for c in range(0, WIDTH, 512):
        partial[:, c : c + 512] = dot(normed[...], weight[:, c : c + 512]).astype(BF16)
    for n, out in enumerate((out_0, out_1, out_2, out_3)):
        first = pl.multiple_of(lax.rem(index[0] + n, N_TP) * 128, 128)
        out[...] = partial[pl.ds(first, 128), :]


def mixer_state(keys, values, log_input_gate, forget_gate_logits, extra_log_decay):
    log_forget = jax.nn.log_sigmoid(forget_gate_logits) + extra_log_decay
    return pl.pallas_call(
        state_body,
        out_shape=(
            jax.ShapeDtypeStruct((N_EP, 16, PIECE), BF16),
            jax.ShapeDtypeStruct((8, TOK), F32),
        ),
        compiler_params=PARAMS,
        name="local_state",
    )(keys, values, log_input_gate, log_forget)


def mixer_prefix(index, arrived):
    return pl.pallas_call(
        prefix_body,
        in_specs=[
            pl.BlockSpec(memory_space=pltpu.SMEM),
            pl.BlockSpec(memory_space=pltpu.VMEM),
        ],
        out_shape=(
            jax.ShapeDtypeStruct((N_EP, 16, 128), BF16),
            jax.ShapeDtypeStruct((8, 128), F32),
        ),
        compiler_params=PARAMS,
        name="prefix",
    )(index, in_vmem(arrived))


def mixer_cells(index, queries, keys, values, gaps, prefix, level, gain, weight):
    vmem = pl.BlockSpec(memory_space=pltpu.VMEM)
    return pl.pallas_call(
        cell_body,
        in_specs=[pl.BlockSpec(memory_space=pltpu.SMEM)] + [vmem] * 8,
        out_specs=[vmem] * 4,
        out_shape=[jax.ShapeDtypeStruct((128, WIDTH), BF16)] * 4,
        scratch_shapes=[pltpu.VMEM((TOK, 2 * VAL), BF16), pltpu.VMEM((TOK, WIDTH), BF16)],
        compiler_params=PARAMS,
        name="cells",
    )(index, queries, keys, values, gaps, in_vmem(prefix), level, gain.reshape(1, -1), weight)


def dispatch_body(rows, gain, routes, scores, state, outgoing, select, stacked, slots):
    inputs = rows[...].astype(F32)
    scale = lax.rsqrt(jnp.mean(inputs * inputs, axis=1, keepdims=True) + EPSILON)
    normed = (inputs * scale * gain[...]).astype(BF16)
    for c in range(PIECES):
        stacked[c * ROWS : (c + 1) * ROWS, :] = normed[:, c * PIECE : (c + 1) * PIECE]
    expert = iota((EXPERTS, ROWS), 0)
    hits = [routes[p : p + 1] == expert for p in range(3)]
    named = hits[0] | hits[1] | hits[2]
    before = (iota((ROWS, ROWS), 0) < iota((ROWS, ROWS), 1)).astype(F32).astype(BF16)
    rank = dot(named.astype(F32).astype(BF16), before)
    place = jnp.where(named, rank, -1.0).astype(BF16)
    share = scores[...] / jnp.sum(scores[...], axis=0, keepdims=True)
    shares = sum(jnp.where(hits[p], share[p : p + 1], 0.0) for p in range(3)).astype(BF16)
    wide = PIECES * ROWS
    repeat = (iota((ROWS, wide), 0) == (iota((ROWS, wide), 1) & (ROWS - 1))).astype(F32).astype(BF16)
    slots[...] = dot(place, repeat)
    row, col = iota((MSG, wide), 0), iota((MSG, wide), 1)
    piece = sum((row >= n * CAP).astype(jnp.int32) for n in range(1, PIECES))
    pattern = jnp.where((col >> 6) == piece, row - CAP * piece, -7).astype(F32)

    def one_group(g, carry):
        picks = []
        for e in range(GROUP):
            mine = slots[pl.ds(g * GROUP + e, 1), :]
            picks.append((jnp.broadcast_to(mine, (MSG, wide)) == pattern).astype(F32).astype(BF16))
        picked = dot(jnp.concatenate(picks, axis=0), stacked[...]).reshape(GROUP, MSG, PIECE)
        extra = state[pl.ds(g * GROUP, GROUP)].astype(F32)
        outgoing[pl.ds(g * GROUP, GROUP)] = jnp.concatenate([picked, extra], axis=1).astype(BF16)
        return carry

    lax.fori_loop(0, EXPERTS // GROUP, one_group, 0)
    same = (iota((ROWS, ROWS), 0) == iota((ROWS, ROWS), 1)).astype(F32).astype(BF16)
    spread, slot, _ = message_columns()
    long_place = dot(dot_nt(same, place).astype(BF16), spread)
    long_share = dot(dot_nt(same, shares).astype(BF16), spread)
    select[...] = jnp.where(long_place == slot, long_share, 0.0).astype(BF16)


def message_columns():
    long = EXPERTS * MSG
    offset = iota((EXPERTS, long), 1) - iota((EXPERTS, long), 0) * MSG
    inside = (offset >= 0) & (offset < MSG)
    within = jnp.sum(jnp.where(inside, offset.astype(F32), 0.0), axis=0, keepdims=True)
    piece = sum((within >= n * CAP).astype(F32) for n in range(1, PIECES))
    return inside.astype(F32).astype(BF16), within - CAP * piece, piece


def turn_matrix(pieces, back):
    size = GROUP * CAP * pieces
    own, other = (1, 0) if back else (0, 1)
    line = iota((1, size) if back else (size, 1), own)
    piece = sum((line >= n * MSG).astype(jnp.int32) for n in range(1, pieces))
    line = line - MSG * piece
    source = sum((line >= n * CAP).astype(jnp.int32) for n in range(1, GROUP))
    place = source * (CAP * pieces) + piece * CAP + line - CAP * source
    return (iota((size, size), other) == place).astype(F32).astype(BF16)


def gated(rows, both):
    products = dot(rows, both)
    return (jax.nn.silu(products[:, :QUARTER]) * products[:, QUARTER:]).astype(BF16)


def hidden_near_body(arrived, *refs):
    weights, (hidden, rows, loaded, done) = refs[:6], refs[6:]
    copies = []
    for n, weight in enumerate(weights):
        lanes = pl.ds((n % 2) * QUARTER, QUARTER)
        copies.append(pltpu.make_async_copy(weight, loaded.at[n // 2, :, lanes], done.at[n]))
    for copy in copies:
        copy.start()
    order = turn_matrix(PIECES, False)
    for g in range(N_EP // GROUP):
        block = arrived[g * GROUP : (g + 1) * GROUP, :MSG].reshape(GROUP * MSG, PIECE)
        turned = dot(order, block).astype(BF16)
        for c in range(PIECES):
            rows[g * MSG : (g + 1) * MSG, c * PIECE : (c + 1) * PIECE] = turned[c * MSG : (c + 1) * MSG]
    for q in range(3):
        copies[2 * q].wait()
        copies[2 * q + 1].wait()
        hidden[:, q * QUARTER : (q + 1) * QUARTER] = gated(rows[...], loaded[q])


def hidden_far_body(rows, gate, up, hidden):
    hidden[...] = gated(rows[...], jnp.concatenate([gate[...], up[...]], axis=1))


def down_near_body(hidden, out, *refs):
    ups_of, downs_of = refs[:BLOCKS], refs[BLOCKS : 2 * BLOCKS]
    partial_low, partial_high, loaded, done = refs[2 * BLOCKS :]
    copies = []
    for n in range(BLOCKS):
        rows = pl.ds(n * PART, PART)
        for q, source in enumerate((out.at[rows], ups_of[n], downs_of[n])):
            target = loaded.at[rows, pl.ds(q * QUARTER, QUARTER)]
            copies.append(pltpu.make_async_copy(source, target, done.at[3 * n + q]))
    for copy in copies:
        copy.start()
    half = WIDTH // 2
    for part, partial in enumerate((partial_low, partial_high)):
        for copy in copies[6 * part : 6 * part + 6]:
            copy.wait()
        partial[...] = dot_nt(hidden[...], loaded[part * half : (part + 1) * half, :])


def far_messages(hidden, partial, w_a, w_b, result, lines):
    order = turn_matrix(PIECES // 2, True)
    far = jnp.concatenate([dot_nt(hidden[...], w_a[...]), dot_nt(hidden[...], w_b[...])], axis=1)
    total = (partial[...] + far).astype(BF16)
    for g in range(N_EP // GROUP):
        block = total[g * MSG : (g + 1) * MSG]
        pieces = [block[:, c * PIECE : (c + 1) * PIECE] for c in range(PIECES // 2)]
        turned = dot(order, jnp.concatenate(pieces, axis=0)).astype(BF16)
        result[g * GROUP : (g + 1) * GROUP, lines] = turned.reshape(GROUP, MSG // 2, PIECE)


def down_low_body(hidden, partial, w_a, w_b, result):
    far_messages(hidden, partial, w_a, w_b, result, slice(0, MSG // 2))


def down_high_body(hidden, partial, w_a, w_b, low, result):
    result[:, : MSG // 2] = low[...]
    far_messages(hidden, partial, w_a, w_b, result, slice(MSG // 2, MSG))


def spread_body(select, shares):
    _, _, piece = message_columns()
    base = select[...].astype(F32)
    for c in range(PIECES):
        shares[c * ROWS : (c + 1) * ROWS, :] = jnp.where(piece == c, base, 0.0).astype(BF16)


def combine_body(shares, returned, out):
    long = EXPERTS * MSG
    rows = returned[...].reshape(long, PIECE)
    middle = long // 2
    total = dot(shares[:, :middle], rows[:middle]) + dot(shares[:, middle:], rows[middle:])
    total = total.astype(BF16)
    for c in range(PIECES):
        out[:, c * PIECE : (c + 1) * PIECE] = total[c * ROWS : (c + 1) * ROWS]


def dispatch(rows, gain, routes, scores, state):
    return pl.pallas_call(
        dispatch_body,
        out_shape=(
            jax.ShapeDtypeStruct((EXPERTS, MSG + 16, PIECE), BF16),
            jax.ShapeDtypeStruct((ROWS, EXPERTS * MSG), BF16),
        ),
        scratch_shapes=[
            pltpu.VMEM((PIECES * ROWS, PIECE), BF16),
            pltpu.VMEM((EXPERTS, PIECES * ROWS), F32),
        ],
        compiler_params=PARAMS,
        name="dispatch",
    )(rows, gain.reshape(1, -1), routes.T, scores.T, state)


def hidden_near(arrived, weights):
    vmem = pl.BlockSpec(memory_space=pltpu.VMEM)
    anywhere = pl.BlockSpec(memory_space=pl.ANY)
    return pl.pallas_call(
        hidden_near_body,
        in_specs=[vmem] + [anywhere] * 6,
        out_specs=(vmem, vmem),
        out_shape=(
            pltpu.VMEM((N_EP * CAP, 3 * QUARTER), BF16),
            jax.ShapeDtypeStruct((N_EP * CAP, WIDTH), BF16),
        ),
        scratch_shapes=[
            pltpu.VMEM((3, WIDTH, 2 * QUARTER), BF16),
            pltpu.SemaphoreType.DMA((6,)),
        ],
        compiler_params=PARAMS,
        name="hidden_near",
    )(in_vmem(arrived), *weights)


def hidden_far(rows, gate, up):
    vmem = pl.BlockSpec(memory_space=pltpu.VMEM)
    return pl.pallas_call(
        hidden_far_body,
        in_specs=[vmem] * 3,
        out_specs=vmem,
        out_shape=pltpu.VMEM((N_EP * CAP, QUARTER), BF16),
        compiler_params=SMALL,
        name="hidden_far",
    )(rows, in_vmem(gate), in_vmem(up))


def down_near(hidden, out, ups_of, downs_of):
    vmem = pl.BlockSpec(memory_space=pltpu.VMEM)
    anywhere = pl.BlockSpec(memory_space=pl.ANY)
    return pl.pallas_call(
        down_near_body,
        in_specs=[vmem] + [anywhere] * (1 + 2 * BLOCKS),
        out_specs=(vmem, vmem),
        out_shape=(pltpu.VMEM((N_EP * CAP, WIDTH // 2), F32),) * 2,
        scratch_shapes=[
            pltpu.VMEM((WIDTH, 3 * QUARTER), BF16),
            pltpu.SemaphoreType.DMA((3 * BLOCKS,)),
        ],
        compiler_params=PARAMS,
        name="down_near",
    )(in_vmem(hidden), out, *ups_of, *downs_of)


def down_far(body, lines, *operands):
    vmem = pl.BlockSpec(memory_space=pltpu.VMEM)
    return pl.pallas_call(
        body,
        in_specs=[vmem] * len(operands),
        out_specs=vmem,
        out_shape=pltpu.VMEM((N_EP, lines, PIECE), BF16),
        compiler_params=SMALL,
        name="down_far",
    )(*[in_vmem(x) for x in operands])


def spread_shares(select):
    vmem = pl.BlockSpec(memory_space=pltpu.VMEM)
    return pl.pallas_call(
        spread_body,
        in_specs=[vmem],
        out_specs=vmem,
        out_shape=pltpu.VMEM((PIECES * ROWS, EXPERTS * MSG), BF16),
        compiler_params=SMALL,
        name="spread",
    )(select)


def combine(shares, returned):
    return pl.pallas_call(
        combine_body,
        out_shape=jax.ShapeDtypeStruct((ROWS, WIDTH), BF16),
        compiler_params=SMALL,
        name="combine",
    )(in_vmem(shares), in_vmem(returned))


UP = [(i, (i + 1) % N_TP) for i in range(N_TP)]
DOWN = [(i, (i - 1) % N_TP) for i in range(N_TP)]
ACROSS = [(i, (i + 2) % N_TP) for i in range(N_TP)]


def send(x, ring):
    return lax.ppermute(x, "tp", ring)


def exchange(x):
    return lax.all_to_all(x, EP, split_axis=0, concat_axis=0, tiled=True)


def shards(
    queries,
    mixer_key_rows,
    mixer_value_rows,
    log_input_gate,
    forget_gate_logits,
    extra_log_decay,
    head_norm_gain,
    mixer_output_weight,
    expert_input_rows,
    expert_norm_gain,
    routes,
    router_picked_scores,
    expert_gate_weight,
    expert_up_weight,
    expert_down_weight,
):
    ep_index = lax.axis_index(EP).astype(jnp.int32).reshape(1)
    tp_index = lax.axis_index("tp").astype(jnp.int32).reshape(1)
    gate, up, out = expert_gate_weight[0], expert_up_weight[0], expert_down_weight[0]

    gates = [gate, send(gate, UP), send(gate, DOWN)]
    ups = [up, send(up, UP), send(up, DOWN)]
    gates.append(send(gates[1], UP))
    ups.append(send(ups[2], DOWN))
    ups_of, downs_of = [], []
    for n in range(BLOCKS):
        block = out[n * PART : (n + 1) * PART]
        ups_of.append(send(block, UP))
        downs_of.append(send(block, DOWN))
    far_outs = [send(downs_of[n], DOWN) if n % 2 else send(ups_of[n], UP) for n in range(BLOCKS)]

    state, gaps = mixer_state(
        mixer_key_rows, mixer_value_rows, log_input_gate, forget_gate_logits, extra_log_decay
    )
    outgoing, select = dispatch(
        expert_input_rows, expert_norm_gain, routes, router_picked_scores, state
    )
    arrived = exchange(outgoing)
    slices, level = mixer_prefix(ep_index, arrived)
    prefix = exchange(slices)

    near = [w for pair in zip(gates[:3], ups[:3]) for w in pair]
    near_units, rows = hidden_near(arrived, near)
    far_units = hidden_far(rows, gates[3], ups[3])

    own, to_up, to_across, to_down = mixer_cells(
        tp_index,
        queries,
        mixer_key_rows,
        mixer_value_rows,
        gaps,
        prefix,
        level,
        head_norm_gain,
        mixer_output_weight,
    )
    parts = [own, send(to_up, UP), send(to_across, ACROSS), send(to_down, DOWN)]

    partial_low, partial_high = down_near(near_units, out, ups_of, downs_of)
    low = down_far(down_low_body, MSG // 2, far_units, partial_low, *far_outs[:2])
    result = down_far(down_high_body, MSG, far_units, partial_high, *far_outs[2:], low)
    returned = exchange(result)
    mixer_output = sum(part.astype(F32) for part in parts).astype(BF16)
    shares = spread_shares(select)
    expert_out = combine(shares, returned)
    return (mixer_output, expert_out)


def solution(mesh):
    split = Mesh(mesh.devices.reshape(8, 4, 2, mesh.shape["tp"]), EP_TP)
    in_specs = (
        P(EP, "tp"),
        P(EP, "tp"),
        P(EP, "tp"),
        P("tp", EP),
        P("tp", EP),
        P("tp", EP),
        P("tp"),
        P("tp", None),
        P(EP_TP, None),
        P(),
        P(EP_TP, None),
        P(EP_TP, None),
        P(EP, None, "tp"),
        P(EP, None, "tp"),
        P(EP, None, "tp"),
    )
    out_specs = (P(EP_TP, None), P(EP_TP, None))

    return jax.shard_map(
        shards, mesh=split, in_specs=in_specs, out_specs=out_specs, check_vma=False
    )
```

time: 370 us -> 212 us (0.57)
  waiting for transfers between devices: 211 us -> 112 us
  local copies, waits for them, and re-layouts: 63.4 us -> 2.9 us
  starting transfers between devices: 22.1 us -> 59.4 us
  Pallas kernels: 0 us -> 33.7 us
  other arithmetic: 32.4 us -> 2.45 us
  matrix products: 23 us -> 0 us
  between operations: 15 us -> 0.84 us
    all_gather x3 -> x0, waiting for transfers between devices: 116 us -> none  [the longest x1 87.1 us: side_by_side(): lax.all_gather(both, axis, axis=dim, tiled=True)]
    ppermute x0 -> x21, waiting for transfers between devices: none -> 106 us  [send(): return lax.ppermute(x, 'tp', ring)]
    all_to_all x2 -> x3, waiting for transfers between devices: 95.1 us -> 5.68 us  [exchange(): return lax.all_to_all(x, EP, split_axis=0, concat_axis=0, tiled=True)]
    pallas_call x0 -> x11, Pallas kernels: none -> 33.7 us  [the longest x1 5.9 us: mixer_cells(): pl.pallas_call(cell_body, in_specs=[pl.BlockSpec(memory_space=pltpu.SMEM)...]
    ppermute x0 -> x21, starting transfers between devices: none -> 26.5 us  [send(): return lax.ppermute(x, 'tp', ring)]
    dot_general x7 -> x0, matrix products: 23 us -> none  [the longest x1 9.93 us: experts_part(): jnp.einsum('ref,edf->red', hidden, full_down, preferred_element_type=jnp....]
    add x20 -> x1, other arithmetic: 13.4 us -> 1.32 us  [mixer_state(): log_forget = jax.nn.log_sigmoid(forget_gate_logits) + extra_log_decay]
    all_to_all x2 -> x3, starting transfers between devices: 21.9 us -> 32.9 us  [exchange(): return lax.all_to_all(x, EP, split_axis=0, concat_axis=0, tiled=True)]
  transfers between devices with their start and end apart: 6 -> 24, of which waited for: 4 -> 8; matrix products, arithmetic and copies ran while one was open for 21% -> 1% of each run, Pallas kernels for 0% -> 11%
where the time goes in v1:
time: 212 us; the launch traced here: 211 us
  waiting for transfers between devices  112 us (53%)
  starting transfers between devices  59.4 us (28%)
  Pallas kernels  33.7 us (16%)
  local copies, waits for them, and re-layouts  2.9 us (1%)
  other arithmetic  2.45 us (1%)
    ppermute x21, waiting for transfers between devices, send(): return lax.ppermute(x, 'tp', ring)  106 us
    all_to_all x3, starting transfers between devices, exchange(): return lax.all_to_all(x, EP, split_axis=0, concat_axis=0, tiled=True)  32.9 us
    ppermute x21, starting transfers between devices, send(): return lax.ppermute(x, 'tp', ring)  26.5 us
    pallas_call x1, Pallas kernels, mixer_cells(): pl.pallas_call(cell_body, in_specs=[pl.BlockSpec(memory_space=pltpu.SMEM)...  5.9 us
    all_to_all x3, waiting for transfers between devices, exchange(): return lax.all_to_all(x, EP, split_axis=0, concat_axis=0, tiled=True)  5.68 us
    pallas_call x1, Pallas kernels, hidden_near(): pl.pallas_call(hidden_near_body, in_specs=[vmem] + [anywhere] * 6, out_sp...  5.45 us
    pallas_call x1, Pallas kernels, dispatch(): pl.pallas_call(dispatch_body, out_shape=(jax.ShapeDtypeStruct((EXPERTS, M...  5.02 us
  transfers between devices with their start and end apart: 24, of which 8 were waited for; matrix products, arithmetic and copies ran while one was open for 1% of the time, Pallas kernels for 11%

profile of v1, /device:TPU:2, one launch (start us, length us, event | category | flops | bytes accessed | tf_op | source)
XLA Modules:
  0.0 210.8 jit_solution(11075972334546973617)
XLA Ops:
  1.9 2.5 %local_state.1 = (bf16[64,16,256]{2,1,0:T(8,128)(2,1)}, f32[8,512]{1,0:T(8,128)}) custom-call(bf16[512,256]{1,0:T(8,128)(2,1)} %keys.3, bf16[512,512]{1,0:T(8,128)(2,1)} %values.3, f32[2,512]{1,0:T(2,128)} %gate_in.1, f32[2,512]{1,0:T(2,128)} %fusion.1.log_forget), custom_call_target="tpu_custom_call" | custom-call | tf_op jit(solution)/shard_map/local_state/pallas_call | solution.py:165
  4.4 5.0 %dispatch.1 = (bf16[64,64,256]{2,1,0:T(8,128)(2,1)}, bf16[64,3072]{1,0:T(8,128)(2,1)}) custom-call(bf16[64,2048]{1,0:T(8,128)(2,1)} %rows.1, f32[1,2048]{1,0:T(1,128)} %bitcast.18, s32[3,64]{1,0:T(4,128)} %bitcast.19, f32[3,64]{1,0:T(4,128)} %bitcast.20, bf16[64,16,256]{2,1,0:T(8,128)(2,1)} %get-tuple-element.17.state), custom_call_target="tpu_custom_call" | custom-call | tf_op jit(solution)/shard_map/dispatch/pallas_call | solution.py:349
  9.5 12.1 %all-to-all-start = ((bf16[64,64,256]{2,1,0:T(8,128)(2,1)}), bf16[64,64,256]{2,1,0:T(8,128)(2,1)S(1)}, u32[]{:S(2)}, u32[]{:S(2)}) async-start(bf16[64,64,256]{2,1,0:T(8,128)(2,1)} %get-tuple-element.18), calls=%async_computation | async-start | bytes 4194304 | tf_op jit(solution)/shard_map/all_to_all | solution.py:456
  26.1 2.9 %collective-permute-start.14 = (bf16[512,256]{1,0:T(8,128)(2,1)S(1)}, bf16[512,256]{1,0:T(8,128)(2,1)S(1)}, u32[]{:S(2)}, u32[]{:S(2)}) collective-permute-start(bf16[512,256]{1,0:T(8,128)(2,1)S(1)} %get-tuple-element.31), channel_id=1, source_target_pairs={{0,3},{1,0},{2,1},{3,2},{4,7},{5,4},{6,5},{7,6},{8,11},{9,8},{10,9... | collective-permute-start | bytes 786440 | tf_op jit(solution)/shard_map/ppermute | solution.py:452
  29.5 24.4 %collective-permute-done.11.refs_2_ = bf16[512,256]{1,0:T(8,128)(2,1)S(1)} collective-permute-done((bf16[512,256]{1,0:T(8,128)(2,1)S(1)}, bf16[512,256]{1,0:T(8,128)(2,1)S(1)}, u32[]{:S(2)}, u32[]{:S(2)}) %collective-permute-start.11) | collective-permute-done | bytes 262176 | tf_op jit(solution)/shard_map/ppermute | solution.py:452
  56.7 2.9 %collective-permute-done.16.refs_7_ = bf16[512,256]{1,0:T(8,128)(2,1)S(1)} collective-permute-done((bf16[512,256]{1,0:T(8,128)(2,1)S(1)}, bf16[512,256]{1,0:T(8,128)(2,1)S(1)}, u32[]{:S(2)}, u32[]{:S(2)}) %collective-permute-start.16) | collective-permute-done | bytes 262176 | tf_op jit(solution)/shard_map/ppermute | solution.py:452
  59.6 3.0 %collective-permute-start.5 = (bf16[2048,256]{1,0:T(8,128)(2,1)}, bf16[2048,256]{1,0:T(8,128)(2,1)}, u32[]{:S(2)}, u32[]{:S(2)}) collective-permute-start(bf16[2048,256]{1,0:T(8,128)(2,1)} %bitcast.6.refs_0_), channel_id=1, source_target_pairs={{0,3},{1,0},{2,1},{3,2},{4,7},{5,4},{6,5},{7,6},{8,11},{9,8},{10,9... | collective-permute-start | bytes 3145736 | tf_op jit(solution)/shard_map/ppermute | solution.py:452
  62.8 3.3 %collective-permute-start.8 = (bf16[2048,256]{1,0:T(8,128)(2,1)}, bf16[2048,256]{1,0:T(8,128)(2,1)}, u32[]{:S(2)}, u32[]{:S(2)}) collective-permute-start(bf16[2048,256]{1,0:T(8,128)(2,1)} %collective-permute-done.6.refs_5_), channel_id=1, source_target_pairs={{0,3},{1,0},{2,1},{3,2},{4,7},{5,4},{6,5},{7,6},{8,11},{9,8},{10,9... | collective-permute-start | bytes 3145736 | tf_op jit(solution)/shard_map/ppermute | solution.py:452
  66.1 47.5 %collective-permute-done.10.refs_1_ = bf16[512,256]{1,0:T(8,128)(2,1)} collective-permute-done((bf16[512,256]{1,0:T(8,128)(2,1)S(1)}, bf16[512,256]{1,0:T(8,128)(2,1)}, u32[]{:S(2)}, u32[]{:S(2)}) %collective-permute-start.10) | collective-permute-done | bytes 262176 | tf_op jit(solution)/shard_map/ppermute | solution.py:452
  113.6 8.0 %collective-permute-done.12.refs_3_ = bf16[512,256]{1,0:T(8,128)(2,1)} collective-permute-done((bf16[512,256]{1,0:T(8,128)(2,1)S(1)}, bf16[512,256]{1,0:T(8,128)(2,1)}, u32[]{:S(2)}, u32[]{:S(2)}) %collective-permute-start.12) | collective-permute-done | bytes 262176 | tf_op jit(solution)/shard_map/ppermute | solution.py:452
  121.6 2.3 %prefix.1 = (bf16[64,16,128]{2,1,0:T(8,128)(2,1)}, f32[8,128]{1,0:T(8,128)}) custom-call(s32[1]{0:T(128)} %bitcast.1.index, bf16[64,64,256]{2,1,0:T(8,128)(2,1)S(1)} %all-to-all-done.arrived), custom_call_target="tpu_custom_call" | custom-call | tf_op jit(solution)/shard_map/prefix/pallas_call | solution.py:177
  123.9 10.3 %all-to-all-start.1 = ((bf16[64,16,128]{2,1,0:T(8,128)(2,1)}), bf16[64,16,128]{2,1,0:T(8,128)(2,1)S(1)}, u32[]{:S(2)}, u32[]{:S(2)}) async-start(bf16[64,16,128]{2,1,0:T(8,128)(2,1)} %get-tuple-element.19), calls=%async_computation.1 | async-start | bytes 524288 | tf_op jit(solution)/shard_map/all_to_all | solution.py:456
  134.3 2.1 collective-permute-start.19
  138.5 2.4 %collective-permute-start.18 = (bf16[512,256]{1,0:T(8,128)(2,1)}, bf16[512,256]{1,0:T(8,128)(2,1)}, u32[]{:S(2)}, u32[]{:S(2)}) collective-permute-start(bf16[512,256]{1,0:T(8,128)(2,1)} %copy-done.5), channel_id=1, source_target_pairs={{0,3},{1,0},{2,1},{3,2},{4,7},{5,4},{6,5},{7,6},{8,11},{9,8},{10,9... | collective-permute-start | bytes 786440 | tf_op jit(solution)/shard_map/ppermute | solution.py:452
  140.9 5.4 %hidden_near.1 = (bf16[384,768]{1,0:T(8,128)(2,1)S(1)}, bf16[384,2048]{1,0:T(8,128)(2,1)}) custom-call(bf16[64,64,256]{2,1,0:T(8,128)(2,1)S(1)} %all-to-all-done.arrived, bf16[2048,256]{1,0:T(8,128)(2,1)} %bitcast.6.refs_0_, bf16[2048,256]{1,0:T(8,128)(2,1)} %bitcast.7.refs_1_, bf16[2048,256]{1,0:T(8,128)(2,1)} %collective-permute-done.3.refs_2_, ...), custom_call_target="tpu_custom_call" | custom-call | tf_op jit(solution)/shard_map/hidden_near/pallas_call | solution.py:367
  147.8 2.2 %hidden_far.1.hidden = bf16[384,256]{1,0:T(8,128)(2,1)S(1)} custom-call(bf16[384,2048]{1,0:T(8,128)(2,1)S(1)} %copy-done, bf16[2048,256]{1,0:T(8,128)(2,1)S(1)} %collective-permute-done.7.gate, bf16[2048,256]{1,0:T(8,128)(2,1)} %collective-permute-done.8.up), custom_call_target="tpu_custom_call" | custom-call | tf_op jit(solution)/shard_map/hidden_far/pallas_call | solution.py:386
  150.7 3.1 %down_near.1 = (f32[384,1024]{1,0:T(8,128)S(1)}, f32[384,1024]{1,0:T(8,128)S(1)}) custom-call(bf16[384,768]{1,0:T(8,128)(2,1)S(1)} %get-tuple-element.27.hidden, bf16[2048,256]{1,0:T(8,128)(2,1)} %bitcast.17, bf16[512,256]{1,0:T(8,128)(2,1)} %collective-permute-done.9.refs_0_, bf16[512,256]{1,0:T(8,128)(2,1)} %collective-permute-done.10.refs_1_, ...), custom_call_target="tpu_custom_call" | custom-call | tf_op jit(solution)/shard_map/down_near/pallas_call | solution.py:399
  154.5 2.8 %down_far.3 = bf16[64,48,256]{2,1,0:T(8,128)(2,1)} custom-call(bf16[384,256]{1,0:T(8,128)(2,1)S(1)} %hidden_far.1.hidden, f32[384,1024]{1,0:T(8,128)S(1)} %get-tuple-element.28.partial, bf16[512,256]{1,0:T(8,128)(2,1)S(1)} %collective-permute-done.17.w_a, bf16[512,256]{1,0:T(8,128)(2,1)} %collective-permute-done.18.w_b, bf16[64,24,256]{2,1,0:T(8,128)(2,1)S(1)} %down_far.2.low), custom_call_target="tpu_custom_call" | custom-call | tf_op jit(solution)/shard_map/down_far/pallas_call | solution.py:415
  157.3 10.5 %all-to-all-start.2 = ((bf16[64,48,256]{2,1,0:T(8,128)(2,1)}), bf16[64,48,256]{2,1,0:T(8,128)(2,1)}, u32[]{:S(2)}, u32[]{:S(2)}) async-start(bf16[64,48,256]{2,1,0:T(8,128)(2,1)} %down_far.3), calls=%async_computation.2 | async-start | bytes 3145728 | tf_op jit(solution)/shard_map/all_to_all | solution.py:456
  167.8 5.9 %cells.1 = (bf16[128,2048]{1,0:T(8,128)(2,1)}, bf16[128,2048]{1,0:T(8,128)(2,1)}, bf16[128,2048]{1,0:T(8,128)(2,1)}, bf16[128,2048]{1,0:T(8,128)(2,1)}) custom-call(s32[1]{0:T(128)} %bitcast.index, bf16[512,256]{1,0:T(8,128)(2,1)} %queries.1, bf16[512,256]{1,0:T(8,128)(2,1)} %keys.3, bf16[512,512]{1,0:T(8,128)(2,1)} %values.3, ...), custom_call_target="tpu_custom_call" | custom-call | tf_op jit(solution)/shard_map/cells/pallas_call | solution.py:194
  173.7 1.7 collective-permute-start
  178.8 21.4 %collective-permute-done = bf16[128,2048]{1,0:T(8,128)(2,1)S(1)} collective-permute-done((bf16[128,2048]{1,0:T(8,128)(2,1)}, bf16[128,2048]{1,0:T(8,128)(2,1)S(1)}, u32[]{:S(2)}, u32[]{:S(2)}) %collective-permute-start) | collective-permute-done | bytes 524320 | tf_op jit(solution)/shard_map/ppermute | solution.py:452
  202.0 5.7 %all-to-all-done.2.returned = bf16[64,48,256]{2,1,0:T(8,128)(2,1)} async-done(((bf16[64,48,256]{2,1,0:T(8,128)(2,1)}), bf16[64,48,256]{2,1,0:T(8,128)(2,1)}, u32[]{:S(2)}, u32[]{:S(2)}) %all-to-all-start.2) | async-done | bytes 1572896 | tf_op jit(solution)/shard_map/all_to_all | solution.py:456
  207.7 3.1 %combine.1 = bf16[64,2048]{1,0:T(8,128)(2,1)} custom-call(bf16[512,3072]{1,0:T(8,128)(2,1)S(1)} %spread.1.shares, bf16[64,48,256]{2,1,0:T(8,128)(2,1)} %all-to-all-done.2.returned), custom_call_target="tpu_custom_call" | custom-call | tf_op jit(solution)/shard_map/combine/pallas_call | solution.py:438
  (56 shorter events, 19.3 us)
Async XLA Ops:
  9.5 112.1 %all-to-all-start = ((bf16[64,64,256]{2,1,0:T(8,128)(2,1)}), bf16[64,64,256]{2,1,0:T(8,128)(2,1)S(1)}, u32[]{:S(2)}, u32[]{:S(2)}) async-start(bf16[64,64,256]{2,1,0:T(8,128)(2,1)} %get-tuple-element.18), calls=%async_computation | async-start | bytes 4194304 | tf_op jit(solution)/shard_map/all_to_all | solution.py:456
  21.6 41.0 %collective-permute-start.3 = (bf16[2048,256]{1,0:T(8,128)(2,1)}, bf16[2048,256]{1,0:T(8,128)(2,1)}, u32[]{:S(2)}, u32[]{:S(2)}) collective-permute-start(bf16[2048,256]{1,0:T(8,128)(2,1)} %bitcast.6.refs_0_), channel_id=1, source_target_pairs={{0,1},{1,2},{2,3},{3,0},{4,5},{5,6},{6,7},{7,4},{8,9},{9,10},{10,1... | collective-permute-start | bytes 3145736 | tf_op jit(solution)/shard_map/ppermute | solution.py:452
  23.3 39.5 %collective-permute-start.6 = (bf16[2048,256]{1,0:T(8,128)(2,1)}, bf16[2048,256]{1,0:T(8,128)(2,1)}, u32[]{:S(2)}, u32[]{:S(2)}) collective-permute-start(bf16[2048,256]{1,0:T(8,128)(2,1)} %bitcast.7.refs_1_), channel_id=1, source_target_pairs={{0,3},{1,0},{2,1},{3,2},{4,7},{5,4},{6,5},{7,6},{8,11},{9,8},{10,9... | collective-permute-start | bytes 3145736 | tf_op jit(solution)/shard_map/ppermute | solution.py:452
  25.7 28.3 %collective-permute-start.11 = (bf16[512,256]{1,0:T(8,128)(2,1)S(1)}, bf16[512,256]{1,0:T(8,128)(2,1)S(1)}, u32[]{:S(2)}, u32[]{:S(2)}) collective-permute-start(bf16[512,256]{1,0:T(8,128)(2,1)S(1)} %get-tuple-element.33), channel_id=1, source_target_pairs={{0,1},{1,2},{2,3},{3,0},{4,5},{5,6},{6,7},{7,4},{8,9},{9,10},{10,1... | collective-permute-start | bytes 786440 | tf_op jit(solution)/shard_map/ppermute | solution.py:452
  26.1 29.1 %collective-permute-start.14 = (bf16[512,256]{1,0:T(8,128)(2,1)S(1)}, bf16[512,256]{1,0:T(8,128)(2,1)S(1)}, u32[]{:S(2)}, u32[]{:S(2)}) collective-permute-start(bf16[512,256]{1,0:T(8,128)(2,1)S(1)} %get-tuple-element.31), channel_id=1, source_target_pairs={{0,3},{1,0},{2,1},{3,2},{4,7},{5,4},{6,5},{7,6},{8,11},{9,8},{10,9... | collective-permute-start | bytes 786440 | tf_op jit(solution)/shard_map/ppermute | solution.py:452
  28.9 30.7 %collective-permute-start.16 = (bf16[512,256]{1,0:T(8,128)(2,1)S(1)}, bf16[512,256]{1,0:T(8,128)(2,1)S(1)}, u32[]{:S(2)}, u32[]{:S(2)}) collective-permute-start(bf16[512,256]{1,0:T(8,128)(2,1)S(1)} %get-tuple-element.30), channel_id=1, source_target_pairs={{0,3},{1,0},{2,1},{3,2},{4,7},{5,4},{6,5},{7,6},{8,11},{9,8},{10,9... | collective-permute-start | bytes 786440 | tf_op jit(solution)/shard_map/ppermute | solution.py:452
  54.0 12.1 %collective-permute-start.9 = (bf16[512,256]{1,0:T(8,128)(2,1)}, bf16[512,256]{1,0:T(8,128)(2,1)}, u32[]{:S(2)}, u32[]{:S(2)}) collective-permute-start(bf16[512,256]{1,0:T(8,128)(2,1)} %get-tuple-element.32), channel_id=1, source_target_pairs={{0,1},{1,2},{2,3},{3,0},{4,5},{5,6},{6,7},{7,4},{8,9},{9,10},{10,1... | collective-permute-start | bytes 786440 | tf_op jit(solution)/shard_map/ppermute | solution.py:452
  55.1 79.2 %collective-permute-start.4 = (bf16[2048,256]{1,0:T(8,128)(2,1)}, bf16[2048,256]{1,0:T(8,128)(2,1)}, u32[]{:S(2)}, u32[]{:S(2)}) collective-permute-start(bf16[2048,256]{1,0:T(8,128)(2,1)} %bitcast.7.refs_1_), channel_id=1, source_target_pairs={{0,1},{1,2},{2,3},{3,0},{4,5},{5,6},{6,7},{7,4},{8,9},{9,10},{10,1... | collective-permute-start | bytes 3145736 | tf_op jit(solution)/shard_map/ppermute | solution.py:452
  59.6 76.8 %collective-permute-start.5 = (bf16[2048,256]{1,0:T(8,128)(2,1)}, bf16[2048,256]{1,0:T(8,128)(2,1)}, u32[]{:S(2)}, u32[]{:S(2)}) collective-permute-start(bf16[2048,256]{1,0:T(8,128)(2,1)} %bitcast.6.refs_0_), channel_id=1, source_target_pairs={{0,3},{1,0},{2,1},{3,2},{4,7},{5,4},{6,5},{7,6},{8,11},{9,8},{10,9... | collective-permute-start | bytes 3145736 | tf_op jit(solution)/shard_map/ppermute | solution.py:452
  62.7 75.0 %collective-permute-start.7 = (bf16[2048,256]{1,0:T(8,128)(2,1)}, bf16[2048,256]{1,0:T(8,128)(2,1)S(1)}, u32[]{:S(2)}, u32[]{:S(2)}) collective-permute-start(bf16[2048,256]{1,0:T(8,128)(2,1)} %collective-permute-done.3.refs_2_), channel_id=1, source_target_pairs={{0,1},{1,2},{2,3},{3,0},{4,5},{5,6},{6,7},{7,4},{8,9},{9,10},{10,1... | collective-permute-start | bytes 3145736 | tf_op jit(solution)/shard_map/ppermute | solution.py:452
  62.8 75.7 %collective-permute-start.8 = (bf16[2048,256]{1,0:T(8,128)(2,1)}, bf16[2048,256]{1,0:T(8,128)(2,1)}, u32[]{:S(2)}, u32[]{:S(2)}) collective-permute-start(bf16[2048,256]{1,0:T(8,128)(2,1)} %collective-permute-done.6.refs_5_), channel_id=1, source_target_pairs={{0,3},{1,0},{2,1},{3,2},{4,7},{5,4},{6,5},{7,6},{8,11},{9,8},{10,9... | collective-permute-start | bytes 3145736 | tf_op jit(solution)/shard_map/ppermute | solution.py:452
  66.1 47.5 %collective-permute-start.10 = (bf16[512,256]{1,0:T(8,128)(2,1)S(1)}, bf16[512,256]{1,0:T(8,128)(2,1)}, u32[]{:S(2)}, u32[]{:S(2)}) collective-permute-start(bf16[512,256]{1,0:T(8,128)(2,1)S(1)} %get-tuple-element.31), channel_id=1, source_target_pairs={{0,1},{1,2},{2,3},{3,0},{4,5},{5,6},{6,7},{7,4},{8,9},{9,10},{10,1... | collective-permute-start | bytes 786440 | tf_op jit(solution)/shard_map/ppermute | solution.py:452
  113.6 8.0 %collective-permute-start.12 = (bf16[512,256]{1,0:T(8,128)(2,1)S(1)}, bf16[512,256]{1,0:T(8,128)(2,1)}, u32[]{:S(2)}, u32[]{:S(2)}) collective-permute-start(bf16[512,256]{1,0:T(8,128)(2,1)S(1)} %get-tuple-element.30), channel_id=1, source_target_pairs={{0,1},{1,2},{2,3},{3,0},{4,5},{5,6},{6,7},{7,4},{8,9},{9,10},{10,1... | collective-permute-start | bytes 786440 | tf_op jit(solution)/shard_map/ppermute | solution.py:452
  121.6 12.6 %collective-permute-start.13 = (bf16[512,256]{1,0:T(8,128)(2,1)}, bf16[512,256]{1,0:T(8,128)(2,1)}, u32[]{:S(2)}, u32[]{:S(2)}) collective-permute-start(bf16[512,256]{1,0:T(8,128)(2,1)} %get-tuple-element.32), channel_id=1, source_target_pairs={{0,3},{1,0},{2,1},{3,2},{4,7},{5,4},{6,5},{7,6},{8,11},{9,8},{10,9... | collective-permute-start | bytes 786440 | tf_op jit(solution)/shard_map/ppermute | solution.py:452
  123.9 33.4 %all-to-all-start.1 = ((bf16[64,16,128]{2,1,0:T(8,128)(2,1)}), bf16[64,16,128]{2,1,0:T(8,128)(2,1)S(1)}, u32[]{:S(2)}, u32[]{:S(2)}) async-start(bf16[64,16,128]{2,1,0:T(8,128)(2,1)} %get-tuple-element.19), calls=%async_computation.1 | async-start | bytes 524288 | tf_op jit(solution)/shard_map/all_to_all | solution.py:456
  134.2 15.7 %collective-permute-start.15 = (bf16[512,256]{1,0:T(8,128)(2,1)}, bf16[512,256]{1,0:T(8,128)(2,1)S(1)}, u32[]{:S(2)}, u32[]{:S(2)}) collective-permute-start(bf16[512,256]{1,0:T(8,128)(2,1)} %copy-done.8), channel_id=1, source_target_pairs={{0,3},{1,0},{2,1},{3,2},{4,7},{5,4},{6,5},{7,6},{8,11},{9,8},{10,9... | collective-permute-start | bytes 786440 | tf_op jit(solution)/shard_map/ppermute | solution.py:452
  134.3 19.4 %collective-permute-start.19 = (bf16[512,256]{1,0:T(8,128)(2,1)}, bf16[512,256]{1,0:T(8,128)(2,1)S(1)}, u32[]{:S(2)}, u32[]{:S(2)}) collective-permute-start(bf16[512,256]{1,0:T(8,128)(2,1)} %collective-permute-done.9.refs_0_), channel_id=1, source_target_pairs={{0,1},{1,2},{2,3},{3,0},{4,5},{5,6},{6,7},{7,4},{8,9},{9,10},{10,1... | collective-permute-start | bytes 786440 | tf_op jit(solution)/shard_map/ppermute | solution.py:452
  136.4 17.3 %collective-permute-start.20 = (bf16[512,256]{1,0:T(8,128)(2,1)}, bf16[512,256]{1,0:T(8,128)(2,1)S(1)}, u32[]{:S(2)}, u32[]{:S(2)}) collective-permute-start(bf16[512,256]{1,0:T(8,128)(2,1)} %copy-done.6), channel_id=1, source_target_pairs={{0,3},{1,0},{2,1},{3,2},{4,7},{5,4},{6,5},{7,6},{8,11},{9,8},{10,9... | collective-permute-start | bytes 786440 | tf_op jit(solution)/shard_map/ppermute | solution.py:452
  137.7 16.8 %collective-permute-start.17 = (bf16[512,256]{1,0:T(8,128)(2,1)}, bf16[512,256]{1,0:T(8,128)(2,1)S(1)}, u32[]{:S(2)}, u32[]{:S(2)}) collective-permute-start(bf16[512,256]{1,0:T(8,128)(2,1)} %copy-done.4), channel_id=1, source_target_pairs={{0,1},{1,2},{2,3},{3,0},{4,5},{5,6},{6,7},{7,4},{8,9},{9,10},{10,1... | collective-permute-start | bytes 786440 | tf_op jit(solution)/shard_map/ppermute | solution.py:452
  138.5 16.0 %collective-permute-start.18 = (bf16[512,256]{1,0:T(8,128)(2,1)}, bf16[512,256]{1,0:T(8,128)(2,1)}, u32[]{:S(2)}, u32[]{:S(2)}) collective-permute-start(bf16[512,256]{1,0:T(8,128)(2,1)} %copy-done.5), channel_id=1, source_target_pairs={{0,3},{1,0},{2,1},{3,2},{4,7},{5,4},{6,5},{7,6},{8,11},{9,8},{10,9... | collective-permute-start | bytes 786440 | tf_op jit(solution)/shard_map/ppermute | solution.py:452
  157.3 50.4 %all-to-all-start.2 = ((bf16[64,48,256]{2,1,0:T(8,128)(2,1)}), bf16[64,48,256]{2,1,0:T(8,128)(2,1)}, u32[]{:S(2)}, u32[]{:S(2)}) async-start(bf16[64,48,256]{2,1,0:T(8,128)(2,1)} %down_far.3), calls=%async_computation.2 | async-start | bytes 3145728 | tf_op jit(solution)/shard_map/all_to_all | solution.py:456
  173.7 26.6 %collective-permute-start = (bf16[128,2048]{1,0:T(8,128)(2,1)}, bf16[128,2048]{1,0:T(8,128)(2,1)S(1)}, u32[]{:S(2)}, u32[]{:S(2)}) collective-permute-start(bf16[128,2048]{1,0:T(8,128)(2,1)} %get-tuple-element.22), channel_id=1, source_target_pairs={{0,1},{1,2},{2,3},{3,0},{4,5},{5,6},{6,7},{7,4},{8,9},{9,10},{10,1... | collective-permute-start | bytes 1572872 | tf_op jit(solution)/shard_map/ppermute | solution.py:452
  175.4 24.9 %collective-permute-start.1 = (bf16[128,2048]{1,0:T(8,128)(2,1)}, bf16[128,2048]{1,0:T(8,128)(2,1)S(1)}, u32[]{:S(2)}, u32[]{:S(2)}) collective-permute-start(bf16[128,2048]{1,0:T(8,128)(2,1)} %get-tuple-element.23), channel_id=1, source_target_pairs={{0,2},{1,3},{2,0},{3,1},{4,6},{5,7},{6,4},{7,5},{8,10},{9,11},{10,... | collective-permute-start | bytes 1572872 | tf_op jit(solution)/shard_map/ppermute | solution.py:452
  176.4 24.5 %collective-permute-start.2 = (bf16[128,2048]{1,0:T(8,128)(2,1)}, bf16[128,2048]{1,0:T(8,128)(2,1)S(1)}, u32[]{:S(2)}, u32[]{:S(2)}) collective-permute-start(bf16[128,2048]{1,0:T(8,128)(2,1)} %get-tuple-element.24), channel_id=1, source_target_pairs={{0,3},{1,0},{2,1},{3,2},{4,7},{5,4},{6,5},{7,6},{8,11},{9,8},{10,9... | collective-permute-start | bytes 1572872 | tf_op jit(solution)/shard_map/ppermute | solution.py:452
  (9 other events, 107.1 us)
